TPU v7x, 32 devices: a whole 2x2x4 slice. The times are simulated.
32 devices in a mesh: grp: 2 (over y), fs: 4 (over z), tp: 4 (over x, core).
Axes of the slice: x: 2, y: 2, z: 4, core: 2. Of those that a mesh axis runs over, the one named last changes fastest.
Arguments:
- tokens: bfloat16 [4096, 2048], P(('grp', 'fs', 'tp')), parts along dimension 0, may hold values from -6 to 6
- route_ids: int32 [4096, 8], P(('grp', 'fs', 'tp')), parts along dimension 0, may hold values from 0 to 15, all different within a row; in each aligned block of 128 rows (0 to 127, 128 to 255, ...) at most 96 rows name the same one
- route_scores: float32 [4096, 8], P(('grp', 'fs', 'tp')), parts along dimension 0, may hold values from 0.05 to 1
- norm_gain: float32 [2048], P('fs'), may hold values from 0.1 to 1.9
- expert_gate: float32 [16, 2048, 256], P(None, 'fs', 'tp'), may hold values from -0.125 to 0.125
- expert_up: float32 [16, 2048, 256], P(None, 'fs', 'tp'), may hold values from -0.125 to 0.125
- expert_down: float32 [16, 256, 2048], P(None, 'fs', 'tp'), may hold values from -0.375 to 0.375
- shared_gate: float32 [2048, 256], P('fs', 'tp'), may hold values from -0.125 to 0.125
- shared_up: float32 [2048, 256], P('fs', 'tp'), may hold values from -0.125 to 0.125
- shared_down: float32 [256, 2048], P('fs', 'tp'), may hold values from -0.375 to 0.375
Outputs:
- mixed: bfloat16 [4096, 2048], P(('grp', 'fs', 'tp')), parts along dimension 0
- sampler_gate: bfloat16 [32, 2048, 256], P(('grp', 'fs', 'tp')), parts along dimension 0
- sampler_up: bfloat16 [32, 2048, 256], P(('grp', 'fs', 'tp')), parts along dimension 0
- sampler_down: bfloat16 [32, 256, 2048], P(('grp', 'fs', 'tp')), parts along dimension 0
- sampler_shared_gate: bfloat16 [4096, 256], P(('grp', 'fs')), parts along dimension 0
- sampler_shared_up: bfloat16 [4096, 256], P(('grp', 'fs')), parts along dimension 0
- sampler_shared_down: bfloat16 [512, 2048], P(('grp', 'fs')), parts along dimension 0
There are 2 independent parts, one for each index of `grp`. A program takes and returns all parts, laid end to end along the dimension named above; an argument that names none is the same for every part. Nothing has to cross between parts.
Inputs may be any that keep to these rules, and one draw needn't show every extreme that they name: `route_ids`: each row names 8 different experts. Among the 128 rows of one device no expert is named more than 96 times, a bound that some block reaches.
All inputs are finite; a program needn't handle non-finite values.
Results may differ from a plain program's by a relative error of at most 0.0084.
Values may be sent and summed in bfloat16 or wider, within the bound.
A program may use at most 128 MiB of HBM per device.

v0:
```python
import jax
import jax.numpy as jnp
from jax import lax
from jax.sharding import PartitionSpec as P

EPSILON = 1e-06
route_scale = 2.5


def expert_rows(row_block, w_gate, w_up, w_down):
    gate_rows = jnp.dot(row_block, w_gate, preferred_element_type=jnp.float32)
    up_rows = jnp.dot(row_block, w_up, preferred_element_type=jnp.float32)
    hidden = (jax.nn.silu(gate_rows) * up_rows).astype(jnp.bfloat16)
    return jnp.dot(hidden, w_down, preferred_element_type=jnp.float32).astype(jnp.bfloat16)


def relayout(arrived, fs_count, tp_count):
    tile_rows = arrived.shape[2]
    tile_cols = arrived.shape[3]
    grid = arrived.reshape(fs_count, tp_count, tile_rows, tile_cols)
    grid = jnp.transpose(grid, (0, 2, 1, 3))
    return grid.reshape(1, fs_count * tile_rows, tp_count * tile_cols)


def on_device(
    tokens,
    route_ids,
    route_scores,
    norm_gain,
    expert_gate,
    expert_up,
    expert_down,
    shared_gate,
    shared_up,
    shared_down,
):
    fs_count = lax.axis_size("fs")
    tp_count = lax.axis_size("tp")
    experts = fs_count * tp_count
    gain_col = norm_gain[:, None]
    piece_gate = (gain_col[None] * expert_gate).astype(jnp.bfloat16)
    piece_up = (gain_col[None] * expert_up).astype(jnp.bfloat16)
    piece_down = expert_down.astype(jnp.bfloat16)
    moved = (
        lax.all_to_all(piece_gate[:, None], ("fs", "tp"), split_axis=0, concat_axis=1, tiled=True),
        lax.all_to_all(piece_up[:, None], ("fs", "tp"), split_axis=0, concat_axis=1, tiled=True),
        lax.all_to_all(piece_down[:, None], ("fs", "tp"), split_axis=0, concat_axis=1, tiled=True),
    )
    served_gate = relayout(moved[0], fs_count, tp_count)
    served_up = relayout(moved[1], fs_count, tp_count)
    served_down = relayout(moved[2], fs_count, tp_count)
    tile_gate = (gain_col * shared_gate).astype(jnp.bfloat16)
    tile_up = (gain_col * shared_up).astype(jnp.bfloat16)
    tile_down = shared_down.astype(jnp.bfloat16)
    held_gate, held_up, held_down = (
        lax.all_gather(tile_gate, "tp", axis=1, tiled=True),
        lax.all_gather(tile_up, "tp", axis=1, tiled=True),
        lax.all_gather(tile_down, "tp", axis=1, tiled=True),
    )
    rows_dev = tokens.shape[0]
    width = tokens.shape[1]
    picks = route_ids.shape[1]
    capacity = 3 * rows_dev * picks // (2 * experts)
    widened = tokens.astype(jnp.float32)
    normed = (
        widened * lax.rsqrt(jnp.mean(widened * widened, axis=1, keepdims=True) + EPSILON)
    ).astype(jnp.bfloat16)
    weights = route_scale * route_scores / jnp.sum(route_scores, axis=1, keepdims=True)
    flat_ids = route_ids.reshape(-1)
    onehot = (flat_ids[:, None] == jnp.arange(experts, dtype=jnp.int32)[None, :]).astype(jnp.int32)
    earlier = jnp.cumsum(onehot, axis=0) - onehot
    ranks = jnp.sum(earlier * onehot, axis=1)
    target = flat_ids * capacity + ranks
    outbox = (
        jnp.zeros((experts * capacity, width), jnp.bfloat16)
        .at[target]
        .set(jnp.repeat(normed, picks, axis=0))
    )
    arrived = lax.all_to_all(
        outbox.reshape(experts, capacity, width),
        ("fs", "tp"),
        split_axis=0,
        concat_axis=0,
        tiled=True,
    )
    finished = expert_rows(
        arrived.reshape(-1, width), served_gate[0], served_up[0], served_down[0]
    ).reshape(arrived.shape)
    returned = lax.all_to_all(finished, ("fs", "tp"), split_axis=0, concat_axis=0, tiled=True)
    results = returned.reshape(experts * capacity, width)[target]
    routed = jnp.sum(
        results.reshape(rows_dev, picks, width).astype(jnp.float32) * weights[:, :, None], axis=1
    )
    columns = normed
    gate_part = jnp.dot(
        columns,
        lax.all_gather(held_gate, "fs", axis=0, tiled=True),
        preferred_element_type=jnp.float32,
    )
    up_part = jnp.dot(
        columns,
        lax.all_gather(held_up, "fs", axis=0, tiled=True),
        preferred_element_type=jnp.float32,
    )
    shared_hidden = (jax.nn.silu(gate_part) * up_part).astype(jnp.bfloat16)
    columns = shared_hidden
    shared_term = jnp.dot(
        columns,
        lax.all_gather(held_down, "fs", axis=0, tiled=True),
        preferred_element_type=jnp.float32,
    )
    mixed = (routed + shared_term).astype(jnp.bfloat16)
    return (mixed, served_gate, served_up, served_down, held_gate, held_up, held_down)


def solution(mesh):
    return jax.shard_map(
        on_device,
        mesh=mesh,
        in_specs=(
            P(("grp", "fs", "tp"), None),
            P(("grp", "fs", "tp"), None),
            P(("grp", "fs", "tp"), None),
            P("fs"),
            P(None, "fs", "tp"),
            P(None, "fs", "tp"),
            P(None, "fs", "tp"),
            P("fs", "tp"),
            P("fs", "tp"),
            P("fs", "tp"),
        ),
        out_specs=(
            P(("grp", "fs", "tp"), None),
            P(("grp", "fs", "tp"), None, None),
            P(("grp", "fs", "tp"), None, None),
            P(("grp", "fs", "tp"), None, None),
            P(("grp", "fs"), None),
            P(("grp", "fs"), None),
            P(("grp", "fs"), None),
        ),
        check_vma=False,
    )
```

profile of v0, /device:TPU:11, one launch (start us, length us, event | category | flops | bytes accessed | tf_op | source)
XLA Modules:
  0.0 485.5 jit_solution(11063605218181208656)
XLA Ops:
  7.2 3.8 fusion.10
  11.0 31.1 %all_to_all.37 = bf16[16,1,512,64]{2,3,1,0:T(8,128)(2,1)S(1)} all-to-all(bf16[16,1,512,64]{2,3,1,0:T(8,128)(2,1)S(1)} %get-tuple-element.36), channel_id=1, replica_groups=mesh['grp'=2,'fs'=4,'tp'=4] {'fs','tp'}, dimensions={0} | all-to-all | bytes 2097152 | tf_op jit(solution)/shard_map/all_to_all | solution.py:45
  42.1 5.0 %all-to-all-start.2 = ((bf16[16,1,512,64]{2,3,1,0:T(8,128)(2,1)}), bf16[16,1,512,64]{2,3,1,0:T(8,128)(2,1)S(1)}, u32[]{:S(2)}, u32[]{:S(2)}) async-start(bf16[16,1,512,64]{2,3,1,0:T(8,128)(2,1)} %get-tuple-element.37), calls=%async_computation.2 | async-start | bytes 2097152 | tf_op jit(solution)/shard_map/all_to_all | solution.py:46
  47.1 2.7 convert_bitcast_fusion
  49.9 22.1 %all-to-all-done.2 = bf16[16,1,512,64]{2,3,1,0:T(8,128)(2,1)S(1)} async-done(((bf16[16,1,512,64]{2,3,1,0:T(8,128)(2,1)}), bf16[16,1,512,64]{2,3,1,0:T(8,128)(2,1)S(1)}, u32[]{:S(2)}, u32[]{:S(2)}) %all-to-all-start.2) | async-done | bytes 1048608 | tf_op jit(solution)/shard_map/all_to_all | solution.py:46
  72.0 4.8 all-to-all-start.3
  77.1 4.5 reduce-window.6
  82.7 10.2 %scatter_custom_fusion = bf16[1536,2048]{1,0:T(8,128)(2,1)} fusion(s32[1024]{0:T(1024)S(1)} %bitcast.93, bf16[]{:T(256)} %constant.9.clone.1, bf16[128,2048]{1,0:T(8,128)(2,1)S(1)} %fusion.9), kind=kCustom, calls=%fused_computation.5 | custom fusion | bytes 6815746 | tf_op jit(solution)/shard_map/scatter | solution.py:77
  92.9 8.9 %all-to-all-done.3 = bf16[16,1,64,512]{3,2,1,0:T(8,128)(2,1)} async-done(((bf16[16,1,64,512]{3,2,1,0:T(8,128)(2,1)}), bf16[16,1,64,512]{3,2,1,0:T(8,128)(2,1)}, u32[]{:S(2)}, u32[]{:S(2)}) %all-to-all-start.3) | async-done | bytes 1048608 | tf_op jit(solution)/shard_map/all_to_all | solution.py:47
  101.8 4.8 all-to-all-start
  110.8 2.0 copy.77
  114.0 130.0 %all-to-all-done = bf16[16,96,2048]{2,1,0:T(8,128)(2,1)} async-done(((bf16[16,96,2048]{2,1,0:T(8,128)(2,1)}), bf16[16,96,2048]{2,1,0:T(8,128)(2,1)}, u32[]{:S(2)}, u32[]{:S(2)}) %all-to-all-start) | async-done | bytes 6291488 | tf_op jit(solution)/shard_map/all_to_all | solution.py:79
  244.0 6.1 %fusion.25 = f32[1536,256]{1,0:T(8,128)} fusion(bf16[1536,2048]{1,0:T(8,128)(2,1)} %bitcast.6, bf16[2048,256]{0,1:T(8,128)(2,1)} %bitcast.87), kind=kOutput, calls=%fused_computation.51 | convolution fusion | flops 1610612736 | bytes 8912896 | tf_op jit(solution)/shard_map/dot_general | solution.py:11
  250.1 12.9 %convolution_convert_fusion = bf16[1536,2048]{1,0:T(8,128)(2,1)} fusion(bf16[256,2048]{1,0:T(8,128)(2,1)} %bitcast.89, bf16[1536,2048]{1,0:T(8,128)(2,1)} %bitcast.6, bf16[2048,256]{0,1:T(8,128)(2,1)} %bitcast.88, f32[1536,256]{1,0:T(8,128)} %fusion.25), kind=kOutput, calls=%fused_computation.4 | convolution fusion | flops 3226730496 | bytes 16252928 | tf_op jit(solution)/shard_map/dot_general | solution.py:14
  263.0 4.9 %all-to-all-start.4 = ((bf16[16,96,2048]{2,1,0:T(8,128)(2,1)}), bf16[16,96,2048]{2,1,0:T(8,128)(2,1)}, u32[]{:S(2)}, u32[]{:S(2)}) async-start(bf16[16,96,2048]{2,1,0:T(8,128)(2,1)} %bitcast.84), calls=%async_computation.4 | async-start | bytes 12582912 | tf_op jit(solution)/shard_map/all_to_all | solution.py:89
  268.0 29.8 %all_gather.18 = bf16[512,256]{0,1:T(8,128)(2,1)} all-gather(bf16[512,64]{0,1:T(8,128)(2,1)S(1)} %get-tuple-element.34), channel_id=1, replica_groups=mesh['grp'=2,'fs'=4,'tp'=4] {'tp'}, dimensions={1}, use_global_device_ids=true | all-gather | bytes 327680 | tf_op jit(solution)/shard_map/all_gather | solution.py:56
  298.0 10.4 %all_gather.20 = bf16[512,256]{0,1:T(8,128)(2,1)} all-gather(bf16[512,64]{0,1:T(8,128)(2,1)S(1)} %get-tuple-element.35), channel_id=1, replica_groups=mesh['grp'=2,'fs'=4,'tp'=4] {'tp'}, dimensions={1}, use_global_device_ids=true | all-gather | bytes 327680 | tf_op jit(solution)/shard_map/all_gather | solution.py:57
  309.3 8.1 %all_gather.22 = bf16[64,2048]{1,0:T(8,128)(2,1)} all-gather(bf16[64,512]{1,0:T(8,128)(2,1)S(1)} %convert_element_type.63), channel_id=1, replica_groups=mesh['grp'=2,'fs'=4,'tp'=4] {'tp'}, dimensions={1}, use_global_device_ids=true | all-gather | bytes 327680 | tf_op jit(solution)/shard_map/all_gather | solution.py:58
  321.1 52.7 %all-gather.4.cloned.1.call-done = bf16[2048,256]{0,1:T(8,128)(2,1)} async-done(((bf16[512,256]{0,1:T(8,128)(2,1)}), bf16[2048,256]{0,1:T(8,128)(2,1)}) %all-gather.4.cloned.1.call-update) | async-done | bytes 1048592 | tf_op jit(solution)/shard_map/all_gather | solution.py:97
  377.3 2.3 copy.62
  383.2 72.7 %all-to-all-done.4 = bf16[16,96,2048]{2,1,0:T(8,128)(2,1)} async-done(((bf16[16,96,2048]{2,1,0:T(8,128)(2,1)}), bf16[16,96,2048]{2,1,0:T(8,128)(2,1)}, u32[]{:S(2)}, u32[]{:S(2)}) %all-to-all-start.4) | async-done | bytes 6291488 | tf_op jit(solution)/shard_map/all_to_all | solution.py:89
  455.9 12.4 %gather_fusion = bf16[1024,2048]{1,0:T(8,128)(2,1)} fusion(bf16[1536,2048]{1,0:T(8,128)(2,1)} %bitcast.18, s32[1024]{0:T(1024)S(1)} %broadcast_clamp_fusion), kind=kCustom, calls=%fused_computation | custom fusion | bytes 8392704 | tf_op jit(solution)/shard_map/gather | solution.py:90
  468.4 6.5 %fusion = f32[128,2048]{1,0:T(8,128)S(1)} fusion(bf16[1024,2048]{1,0:T(8,128)(2,1)} %gather_fusion, f32[128,8]{1,0:T(8,128)S(1)} %copy.61), kind=kLoop, calls=%fused_computation.3 | loop fusion | flops 6029312 | bytes 5246976 | tf_op jit(solution)/shard_map/reduce_sum | solution.py:91
  475.0 3.3 fusion.5
  (63 shorter events, 19.4 us)
Async XLA Ops:
  42.1 34.7 %copy-start.6 = (s32[128,8]{0,1:T(8,128)S(1)}, s32[128,8]{0,1:T(8,128)}, u32[]{:S(2)}) copy-start(s32[128,8]{0,1:T(8,128)} %param.11) | copy-start | bytes 12292
  42.1 40.2 %copy-start.3 = (bf16[128,2048]{1,0:T(8,128)(2,1)S(1)}, bf16[128,2048]{1,0:T(8,128)(2,1)}, u32[]{:S(2)}) copy-start(bf16[128,2048]{1,0:T(8,128)(2,1)} %param.10) | copy-start | bytes 1572868
  42.1 29.9 %all-to-all-start.2 = ((bf16[16,1,512,64]{2,3,1,0:T(8,128)(2,1)}), bf16[16,1,512,64]{2,3,1,0:T(8,128)(2,1)S(1)}, u32[]{:S(2)}, u32[]{:S(2)}) async-start(bf16[16,1,512,64]{2,3,1,0:T(8,128)(2,1)} %get-tuple-element.37), calls=%async_computation.2 | async-start | bytes 2097152 | tf_op jit(solution)/shard_map/all_to_all | solution.py:46
  72.0 29.8 %all-to-all-start.3 = ((bf16[16,1,64,512]{3,2,1,0:T(8,128)(2,1)}), bf16[16,1,64,512]{3,2,1,0:T(8,128)(2,1)}, u32[]{:S(2)}, u32[]{:S(2)}) async-start(bf16[16,1,64,512]{3,2,1,0:T(8,128)(2,1)} %convert_bitcast_fusion), calls=%async_computation.3 | async-start | bytes 2097152 | tf_op jit(solution)/shard_map/all_to_all | solution.py:47
  82.7 19.1 %copy-start = (bf16[128,2048]{1,0:T(8,128)(2,1)}, bf16[128,2048]{1,0:T(8,128)(2,1)S(1)}, u32[]{:S(2)}) copy-start(bf16[128,2048]{1,0:T(8,128)(2,1)S(1)} %fusion.9) | copy-start | bytes 1572868
  101.8 142.2 %all-to-all-start = ((bf16[16,96,2048]{2,1,0:T(8,128)(2,1)}), bf16[16,96,2048]{2,1,0:T(8,128)(2,1)}, u32[]{:S(2)}, u32[]{:S(2)}) async-start(bf16[16,96,2048]{2,1,0:T(8,128)(2,1)} %bitcast.77), calls=%async_computation | async-start | bytes 12582912 | tf_op jit(solution)/shard_map/all_to_all | solution.py:79
  263.0 5.0 %copy-start.4 = (f32[512,64]{0,1:T(8,128)S(1)}, f32[512,64]{0,1:T(8,128)}, u32[]{:S(2)}) copy-start(f32[512,64]{0,1:T(8,128)} %param.17) | copy-start | bytes 393220
  263.0 5.0 %copy-start.5 = (f32[512,64]{0,1:T(8,128)S(1)}, f32[512,64]{0,1:T(8,128)}, u32[]{:S(2)}) copy-start(f32[512,64]{0,1:T(8,128)} %param.18) | copy-start | bytes 393220
  263.0 5.0 %copy-start.8 = (f32[512]{0:T(512)S(1)}, f32[512]{0:T(512)}, u32[]{:S(2)}) copy-start(f32[512]{0:T(512)} %param.13) | copy-start | bytes 6148
  263.0 58.0 %copy-start.7 = (f32[128,8]{0,1:T(8,128)S(1)}, f32[128,8]{0,1:T(8,128)}, u32[]{:S(2)}) copy-start(f32[128,8]{0,1:T(8,128)} %param.12) | copy-start | bytes 12292
  263.0 192.9 %all-to-all-start.4 = ((bf16[16,96,2048]{2,1,0:T(8,128)(2,1)}), bf16[16,96,2048]{2,1,0:T(8,128)(2,1)}, u32[]{:S(2)}, u32[]{:S(2)}) async-start(bf16[16,96,2048]{2,1,0:T(8,128)(2,1)} %bitcast.84), calls=%async_computation.4 | async-start | bytes 12582912 | tf_op jit(solution)/shard_map/all_to_all | solution.py:89
  267.9 105.9 %all-gather.4.cloned.1.call-start = ((), (), s32[]{:S(2)}) async-start(), calls=%async_computation.5 | async-start | bytes 1310720 | tf_op jit(solution)/shard_map/all_gather | solution.py:97
  297.9 177.0 %all-gather.6.cloned.1.call-start = ((), (), s32[]{:S(2)}) async-start(), calls=%async_computation.6 | async-start | bytes 1310720 | tf_op jit(solution)/shard_map/all_gather | solution.py:102
  308.3 166.6 %all-gather.8.cloned.1.call-start = ((), (), s32[]{:S(2)}) async-start(), calls=%async_computation.7 | async-start | bytes 1310720 | tf_op jit(solution)/shard_map/all_gather | solution.py:109
  468.4 6.6 %copy-start.1 = (bf16[128,2048]{1,0:T(8,128)(2,1)S(1)}, bf16[128,2048]{1,0:T(8,128)(2,1)}, u32[]{:S(2)}) copy-start(bf16[128,2048]{1,0:T(8,128)(2,1)} %copy-done) | copy-start | bytes 1572868
  468.4 9.9 %copy-start.2 = (bf16[64,2048]{1,0:T(8,128)(2,1)S(1)}, bf16[64,2048]{1,0:T(8,128)(2,1)}, u32[]{:S(2)}) copy-start(bf16[64,2048]{1,0:T(8,128)(2,1)} %all_gather.22) | copy-start | bytes 786436
Sparse Core Ops, SparseCore 0:
  298.0 75.7 all-gather.3
  375.4 37.3 all-gather.5
  414.3 35.7 all-gather.7
where the time goes:
time: 486 us; the launch traced here: 485 us
  waiting for transfers between devices  287 us (59%)
  blocking collectives  79.3 us (16%)
  local copies, waits for them, and re-layouts  42.8 us (9%)
  matrix products  24.1 us (5%)
  starting transfers between devices  19.7 us (4%)
  other arithmetic  19.1 us (4%)
  between operations  13.9 us (3%)
    all_to_all x1, waiting for transfers between devices, on_device(): lax.all_to_all(outbox.reshape(experts, capacity, width), ('fs', 'tp'), sp...  130 us
    all_to_all x1, waiting for transfers between devices, on_device(): lax.all_to_all(finished, ('fs', 'tp'), split_axis=0, concat_axis=0, tiled...  72.7 us
    all_gather x1, waiting for transfers between devices, on_device(): lax.all_gather(held_gate, 'fs', axis=0, tiled=True)  52.7 us
    all_to_all x1, blocking collectives, on_device(): lax.all_to_all(piece_gate[:, None], ('fs', 'tp'), split_axis=0, concat_ax...  31.1 us
    all_gather x1, blocking collectives, on_device(): lax.all_gather(tile_gate, 'tp', axis=1, tiled=True)  29.8 us
    all_to_all x1, waiting for transfers between devices, on_device(): lax.all_to_all(piece_up[:, None], ('fs', 'tp'), split_axis=0, concat_axis...  22.1 us
    dot_general x1, matrix products, expert_rows(): jnp.dot(hidden, w_down, preferred_element_type=jnp.float32)  12.9 us
    gather x1, local copies, waits for them, and re-layouts, on_device(): results = returned.reshape(experts * capacity, width)[target]  12.4 us
  transfers between devices with their start and end apart: 7, of which 5 were waited for; matrix products, arithmetic and copies ran while one was open for 12% of the time, Pallas kernels for 0%

commit v1 on v0

--- a/solution.py
+++ b/solution.py
@@ -22,7 +22,7 @@
     return grid.reshape(1, fs_count * tile_rows, tp_count * tile_cols)
 
 
-def on_device(
+def dispatch_plan(
     tokens,
     route_ids,
     route_scores,
@@ -113,6 +113,89 @@
     return (mixed, served_gate, served_up, served_down, held_gate, held_up, held_down)
 
 
+def dense_plan(
+    tokens,
+    route_ids,
+    route_scores,
+    norm_gain,
+    expert_gate,
+    expert_up,
+    expert_down,
+    shared_gate,
+    shared_up,
+    shared_down,
+):
+    fs_count = lax.axis_size("fs")
+    tp_count = lax.axis_size("tp")
+    experts = fs_count * tp_count
+    both = ("fs", "tp")
+    rows_dev, width = tokens.shape
+    widened = tokens.astype(jnp.float32)
+    normed = (
+        widened * lax.rsqrt(jnp.mean(widened * widened, axis=1, keepdims=True) + EPSILON)
+    ).astype(jnp.bfloat16)
+    weights = route_scale * route_scores / jnp.sum(route_scores, axis=1, keepdims=True)
+    named = route_ids[:, :, None] == jnp.arange(experts, dtype=jnp.int32)[None, None, :]
+    shares = jnp.sum(jnp.where(named, weights[:, :, None], 0.0), axis=1)
+    all_normed = lax.all_gather(normed, both, axis=0, tiled=True)
+    own_share = lax.all_to_all(
+        shares.T.reshape(experts, 1, rows_dev), both, split_axis=0, concat_axis=1, tiled=True
+    ).reshape(-1)
+
+    gain_col = norm_gain[:, None]
+    piece_gate = (gain_col[None] * expert_gate).astype(jnp.bfloat16)
+    piece_up = (gain_col[None] * expert_up).astype(jnp.bfloat16)
+    piece_pair = jnp.concatenate([piece_gate, piece_up], axis=2)
+    piece_down = expert_down.astype(jnp.bfloat16)
+    pair = lax.all_to_all(piece_pair[:, None], both, split_axis=0, concat_axis=1, tiled=True)
+    down = lax.all_to_all(piece_down[:, None], both, split_axis=0, concat_axis=1, tiled=True)
+    cols = expert_gate.shape[2]
+    served_gate = relayout(pair[:, :, :, :cols], fs_count, tp_count)
+    served_up = relayout(pair[:, :, :, cols:], fs_count, tp_count)
+    served_down = relayout(down, fs_count, tp_count)
+    tile_gate = (gain_col * shared_gate).astype(jnp.bfloat16)
+    tile_up = (gain_col * shared_up).astype(jnp.bfloat16)
+    tile_down = shared_down.astype(jnp.bfloat16)
+    held_gate, held_up, held_down = (
+        lax.all_gather(tile_gate, "tp", axis=1, tiled=True),
+        lax.all_gather(tile_up, "tp", axis=1, tiled=True),
+        lax.all_gather(tile_down, "tp", axis=1, tiled=True),
+    )
+    gate_rows = jnp.dot(all_normed, served_gate[0], preferred_element_type=jnp.float32)
+    up_rows = jnp.dot(all_normed, served_up[0], preferred_element_type=jnp.float32)
+    hidden = (jax.nn.silu(gate_rows) * up_rows).astype(jnp.bfloat16)
+    produced = jnp.dot(hidden, served_down[0], preferred_element_type=jnp.float32)
+    partial = (produced * own_share[:, None]).astype(jnp.bfloat16)
+    routed = lax.psum_scatter(partial, both, scatter_dimension=0, tiled=True)
+
+    gate_part = jnp.dot(
+        normed,
+        lax.all_gather(held_gate, "fs", axis=0, tiled=True),
+        preferred_element_type=jnp.float32,
+    )
+    up_part = jnp.dot(
+        normed,
+        lax.all_gather(held_up, "fs", axis=0, tiled=True),
+        preferred_element_type=jnp.float32,
+    )
+    shared_hidden = (jax.nn.silu(gate_part) * up_part).astype(jnp.bfloat16)
+    shared_term = jnp.dot(
+        shared_hidden,
+        lax.all_gather(held_down, "fs", axis=0, tiled=True),
+        preferred_element_type=jnp.float32,
+    )
+    mixed = (routed.astype(jnp.float32) + shared_term).astype(jnp.bfloat16)
+    return (mixed, served_gate, served_up, served_down, held_gate, held_up, held_down)
+
+
+def on_device(*args):
+    experts = lax.axis_size("fs") * lax.axis_size("tp")
+    picks = args[1].shape[1]
+    if experts <= 4 * picks:
+        return dense_plan(*args)
+    return dispatch_plan(*args)
+
+
 def solution(mesh):
     return jax.shard_map(
         on_device,

time: 486 us -> 348 us (0.72)
  waiting for transfers between devices: 287 us -> 225 us
  blocking collectives: 79.3 us -> 37.5 us
  local copies, waits for them, and re-layouts: 42.8 us -> 16.9 us
  other arithmetic: 19.1 us -> 9.88 us
    all_to_all x4 -> x3, waiting for transfers between devices: 234 us -> 75.6 us  [the longest x1 37.9 us: dense_plan(): lax.all_to_all(piece_down[:, None], both, split_axis=0, concat_axis=1, ti...]
    reduce_scatter x0 -> x1, waiting for transfers between devices: none -> 107 us  [dense_plan(): routed = lax.psum_scatter(partial, both, scatter_dimension=0, tiled=True)]
    all_to_all x1 -> x0, blocking collectives: 31.1 us -> none  [on_device(): lax.all_to_all(piece_gate[:, None], ('fs', 'tp'), split_axis=0, concat_ax...]
    gather x1 -> x0, local copies, waits for them, and re-layouts: 12.4 us -> none  [on_device(): results = returned.reshape(experts * capacity, width)[target]]
    all_gather x3 -> x4, waiting for transfers between devices: 52.7 us -> 41.4 us  [the longest x1 28.8 us: dense_plan(): lax.all_gather(held_down, 'fs', axis=0, tiled=True)]
    all_gather x3, blocking collectives: 48.2 us -> 37.5 us  [the longest x1 20.2 us: dense_plan(): lax.all_gather(tile_gate, 'tp', axis=1, tiled=True)]
    scatter x1 -> x0, local copies, waits for them, and re-layouts: 10.2 us -> none  [on_device(): outbox = jnp.zeros((experts * capacity, width), jnp.bfloat16).at[target]....]
    all_to_all x4 -> x3, starting transfers between devices: 19.6 us -> 16.3 us  [the longest x1 6.65 us: dense_plan(): lax.all_to_all(piece_down[:, None], both, split_axis=0, concat_axis=1, ti...]
  transfers between devices with their start and end apart: 7 -> 8, of which waited for: 5 -> 5; matrix products, arithmetic and copies ran while one was open for 12% -> 13% of each run, Pallas kernels for 0% -> 0%
where the time goes in v1:
time: 348 us; the launch traced here: 346 us
  waiting for transfers between devices  225 us (65%)
  blocking collectives  37.5 us (11%)
  matrix products  26.6 us (8%)
  local copies, waits for them, and re-layouts  16.9 us (5%)
  starting transfers between devices  16.7 us (5%)
  between operations  14 us (4%)
  other arithmetic  9.88 us (3%)
    reduce_scatter x1, waiting for transfers between devices, dense_plan(): routed = lax.psum_scatter(partial, both, scatter_dimension=0, tiled=True)  107 us
    all_to_all x1, waiting for transfers between devices, dense_plan(): lax.all_to_all(piece_down[:, None], both, split_axis=0, concat_axis=1, ti...  37.9 us
    all_to_all x1, waiting for transfers between devices, dense_plan(): lax.all_to_all(piece_pair[:, None], both, split_axis=0, concat_axis=1, ti...  37.7 us
    all_gather x1, waiting for transfers between devices, dense_plan(): lax.all_gather(held_down, 'fs', axis=0, tiled=True)  28.8 us
    all_gather x1, blocking collectives, dense_plan(): lax.all_gather(tile_gate, 'tp', axis=1, tiled=True)  20.2 us
    dot_general x1, matrix products, dense_plan(): jnp.dot(hidden, served_down[0], preferred_element_type=jnp.float32)  13.9 us
    all_gather x1, waiting for transfers between devices, dense_plan(): lax.all_gather(held_up, 'fs', axis=0, tiled=True)  12.6 us
    unnamed x30, local copies, waits for them, and re-layouts  9.78 us
  transfers between devices with their start and end apart: 8, of which 5 were waited for; matrix products, arithmetic and copies ran while one was open for 13% of the time, Pallas kernels for 0%

profile of v1, /device:TPU:11, one launch (start us, length us, event | category | flops | bytes accessed | tf_op | source)
XLA Modules:
  0.0 346.0 jit_solution(2192507976946135979)
XLA Ops:
  7.2 1.4 fusion.3
  8.6 2.0 fusion.4
  11.8 6.7 %all-to-all-start.1 = ((bf16[16,1,64,512]{3,2,1,0:T(8,128)(2,1)}), bf16[16,1,64,512]{3,2,1,0:T(8,128)(2,1)S(1)}, u32[]{:S(2)}, u32[]{:S(2)}) async-start(bf16[16,1,64,512]{3,2,1,0:T(8,128)(2,1)} %convert_bitcast_fusion), calls=%async_computation.1 | async-start | bytes 2097152 | tf_op jit(solution)/shard_map/all_to_all | solution.py:151
  18.4 2.3 multiply_convert_fusion.2
  20.7 1.5 maximum_bitcast_fusion
  22.3 37.9 %all-to-all-done.1 = bf16[16,1,64,512]{3,2,1,0:T(8,128)(2,1)S(1)} async-done(((bf16[16,1,64,512]{3,2,1,0:T(8,128)(2,1)}), bf16[16,1,64,512]{3,2,1,0:T(8,128)(2,1)S(1)}, u32[]{:S(2)}, u32[]{:S(2)}) %all-to-all-start.1) | async-done | bytes 1048608 | tf_op jit(solution)/shard_map/all_to_all | solution.py:151
  60.1 4.8 %all-to-all-start = ((bf16[16,1,512,128]{2,3,1,0:T(8,128)(2,1)}), bf16[16,1,512,128]{2,3,1,0:T(8,128)(2,1)S(1)}, u32[]{:S(2)}, u32[]{:S(2)}) async-start(bf16[16,1,512,128]{2,3,1,0:T(8,128)(2,1)} %maximum_bitcast_fusion), calls=%async_computation | async-start | bytes 4194304 | tf_op jit(solution)/shard_map/all_to_all | solution.py:150
  65.0 20.2 %all_gather.22 = bf16[512,256]{0,1:T(8,128)(2,1)} all-gather(bf16[512,64]{0,1:T(8,128)(2,1)S(1)} %get-tuple-element.43), channel_id=1, replica_groups=mesh['grp'=2,'fs'=4,'tp'=4] {'tp'}, dimensions={1}, use_global_device_ids=true | all-gather | bytes 327680 | tf_op jit(solution)/shard_map/all_gather | solution.py:160
  85.3 9.1 %all_gather.24 = bf16[512,256]{0,1:T(8,128)(2,1)} all-gather(bf16[512,64]{0,1:T(8,128)(2,1)S(1)} %get-tuple-element.44), channel_id=1, replica_groups=mesh['grp'=2,'fs'=4,'tp'=4] {'tp'}, dimensions={1}, use_global_device_ids=true | all-gather | bytes 327680 | tf_op jit(solution)/shard_map/all_gather | solution.py:161
  95.4 8.2 %all_gather.26 = bf16[64,2048]{1,0:T(8,128)(2,1)} all-gather(bf16[64,512]{1,0:T(8,128)(2,1)S(1)} %convert_element_type.50), channel_id=1, replica_groups=mesh['grp'=2,'fs'=4,'tp'=4] {'tp'}, dimensions={1}, use_global_device_ids=true | all-gather | bytes 327680 | tf_op jit(solution)/shard_map/all_gather | solution.py:162
  104.3 2.1 copy.68
  107.6 37.7 %all-to-all-done = bf16[16,1,512,128]{2,3,1,0:T(8,128)(2,1)S(1)} async-done(((bf16[16,1,512,128]{2,3,1,0:T(8,128)(2,1)}), bf16[16,1,512,128]{2,3,1,0:T(8,128)(2,1)S(1)}, u32[]{:S(2)}, u32[]{:S(2)}) %all-to-all-start) | async-done | bytes 2097184 | tf_op jit(solution)/shard_map/all_to_all | solution.py:150
  145.3 4.9 %all-to-all-start.2 = ((f32[16,1,128]{2,1,0:T(1,128)}), f32[16,1,128]{2,1,0:T(1,128)S(1)}, u32[]{:S(2)}, u32[]{:S(2)}) async-start(f32[16,1,128]{2,1,0:T(1,128)} %bitcast.11), calls=%async_computation.2 | async-start | bytes 16384 | tf_op jit(solution)/shard_map/all_to_all | solution.py:141
  154.8 7.4 %fusion.15 = f32[2048,256]{1,0:T(8,128)} fusion(bf16[2048,2048]{1,0:T(8,128)(2,1)} %all-gather.5.cloned.1.call-done, bf16[2048,256]{0,1:T(8,128)(2,1)} %bitcast.62), kind=kOutput, calls=%fused_computation.34 | convolution fusion | flops 2147483648 | bytes 11534336 | tf_op jit(solution)/shard_map/dot_general | solution.py:164
  162.2 13.9 %multiply_convert_fusion = bf16[2048,2048]{1,0:T(8,128)(2,1)} fusion(bf16[256,2048]{1,0:T(8,128)(2,1)} %bitcast.60, f32[2048]{0:T(1024)S(1)} %bitcast.63, bf16[2048,2048]{1,0:T(8,128)(2,1)} %all-gather.5.cloned.1.call-done, bf16[2048,256]{0,1:T(8,128)(2,1)} %bitcast.61, f32[2048,256]{1,0:T(8,128)} %fusion.15), kind=kOutput, calls=%fused_computation | convolution fusion | flops 4306501632 | bytes 20979712 | tf_op jit(solution)/shard_map/dot_general | solution.py:167
  176.1 1.8 copy.57
  178.7 1.9 fusion.16
  180.7 1.6 reshape.66
  183.1 1.3 copy.55
  185.2 1.3 copy.56
  186.5 12.6 %all-gather.9.cloned.1.call-done = bf16[2048,256]{0,1:T(8,128)(2,1)} async-done(((bf16[512,256]{0,1:T(8,128)(2,1)}), bf16[2048,256]{0,1:T(8,128)(2,1)}) %all-gather.9.cloned.1.call-update) | async-done | bytes 1048592 | tf_op jit(solution)/shard_map/all_gather | solution.py:178
  199.1 28.8 %all-gather.11.cloned.1.call-done = bf16[256,2048]{1,0:T(8,128)(2,1)} async-done(((bf16[64,2048]{1,0:T(8,128)(2,1)}), bf16[256,2048]{1,0:T(8,128)(2,1)}) %all-gather.11.cloned.1.call-update) | async-done | bytes 1048592 | tf_op jit(solution)/shard_map/all_gather | solution.py:184
  227.9 107.4 %reduce-scatter.2.cloned.1.call-done = bf16[128,2048]{1,0:T(8,128)(2,1)} async-done(((bf16[2048,2048]{1,0:T(8,128)(2,1)}), bf16[128,2048]{1,0:T(8,128)(2,1)}) %reduce-scatter.2.cloned.1.call-update) | async-done | bytes 524304 | tf_op jit(solution)/shard_map/reduce_scatter | solution.py:169
  335.3 3.4 fusion.1
  (52 shorter events, 11.9 us)
Async XLA Ops:
  7.2 3.5 copy-start.4
  7.2 147.6 %all-gather.5.cloned.1.call-start = ((), (), s32[]{:S(2)}) async-start(), calls=%async_computation.4 | async-start | bytes 8912896 | tf_op jit(solution)/shard_map/all_gather | solution.py:140
  10.6 7.8 %copy-start.9 = (f32[512]{0:T(512)S(1)}, f32[512]{0:T(512)}, u32[]{:S(2)}) copy-start(f32[512]{0:T(512)} %param.13) | copy-start | bytes 6148
  11.8 6.7 %copy-start.5 = (f32[16,512,64]{1,2,0:T(8,128)S(1)}, f32[16,512,64]{1,2,0:T(8,128)}, u32[]{:S(2)}) copy-start(f32[16,512,64]{1,2,0:T(8,128)} %param.14) | copy-start | bytes 6291460
  11.8 48.4 %all-to-all-start.1 = ((bf16[16,1,64,512]{3,2,1,0:T(8,128)(2,1)}), bf16[16,1,64,512]{3,2,1,0:T(8,128)(2,1)S(1)}, u32[]{:S(2)}, u32[]{:S(2)}) async-start(bf16[16,1,64,512]{3,2,1,0:T(8,128)(2,1)} %convert_bitcast_fusion), calls=%async_computation.1 | async-start | bytes 2097152 | tf_op jit(solution)/shard_map/all_to_all | solution.py:151
  22.3 42.7 %copy-start.6 = (f32[512,64]{0,1:T(8,128)S(1)}, f32[512,64]{0,1:T(8,128)}, u32[]{:S(2)}) copy-start(f32[512,64]{0,1:T(8,128)} %param.17) | copy-start | bytes 393220
  22.3 42.7 %copy-start.7 = (f32[512,64]{0,1:T(8,128)S(1)}, f32[512,64]{0,1:T(8,128)}, u32[]{:S(2)}) copy-start(f32[512,64]{0,1:T(8,128)} %param.18) | copy-start | bytes 393220
  60.1 4.9 %copy-start.1 = (bf16[16,1,64,512]{3,2,1,0:T(8,128)(2,1)}, bf16[16,1,64,512]{3,2,1,0:T(8,128)(2,1)S(1)}, u32[]{:S(2)}) copy-start(bf16[16,1,64,512]{3,2,1,0:T(8,128)(2,1)S(1)} %all-to-all-done.1) | copy-start | bytes 3145732
  60.1 85.2 %all-to-all-start = ((bf16[16,1,512,128]{2,3,1,0:T(8,128)(2,1)}), bf16[16,1,512,128]{2,3,1,0:T(8,128)(2,1)S(1)}, u32[]{:S(2)}, u32[]{:S(2)}) async-start(bf16[16,1,512,128]{2,3,1,0:T(8,128)(2,1)} %maximum_bitcast_fusion), calls=%async_computation | async-start | bytes 4194304 | tf_op jit(solution)/shard_map/all_to_all | solution.py:150
  64.9 38.7 %copy-start.8 = (f32[128,8]{0,1:T(8,128)S(1)}, f32[128,8]{0,1:T(8,128)}, u32[]{:S(2)}) copy-start(f32[128,8]{0,1:T(8,128)} %param.12) | copy-start | bytes 12292
  64.9 38.7 %copy-start.10 = (s32[128,8]{0,1:T(8,128)S(1)}, s32[128,8]{0,1:T(8,128)}, u32[]{:S(2)}) copy-start(s32[128,8]{0,1:T(8,128)} %param.11) | copy-start | bytes 12292
  64.9 113.8 %all-gather.7.cloned.1.call-start = ((), (), s32[]{:S(2)}) async-start(), calls=%async_computation.6 | async-start | bytes 1310720 | tf_op jit(solution)/shard_map/all_gather | solution.py:173
  85.3 113.8 %all-gather.9.cloned.1.call-start = ((), (), s32[]{:S(2)}) async-start(), calls=%async_computation.7 | async-start | bytes 1310720 | tf_op jit(solution)/shard_map/all_gather | solution.py:178
  94.4 133.5 %all-gather.11.cloned.1.call-start = ((), (), s32[]{:S(2)}) async-start(), calls=%async_computation.8 | async-start | bytes 1310720 | tf_op jit(solution)/shard_map/all_gather | solution.py:184
  145.3 16.8 %all-to-all-start.2 = ((f32[16,1,128]{2,1,0:T(1,128)}), f32[16,1,128]{2,1,0:T(1,128)S(1)}, u32[]{:S(2)}, u32[]{:S(2)}) async-start(f32[16,1,128]{2,1,0:T(1,128)} %bitcast.11), calls=%async_computation.2 | async-start | bytes 16384 | tf_op jit(solution)/shard_map/all_to_all | solution.py:141
  150.2 185.1 %reduce-scatter.2.cloned.1.call-start = ((), (), s32[]{:S(2)}) async-start(), calls=%async_computation.5 | async-start | bytes 8912896 | tf_op jit(solution)/shard_map/reduce_scatter | solution.py:169
  176.0 1.9 copy-start.3
  184.4 151.0 %copy-start = (bf16[128,2048]{1,0:T(8,128)(2,1)S(1)}, bf16[128,2048]{1,0:T(8,128)(2,1)}, u32[]{:S(2)}) copy-start(bf16[128,2048]{1,0:T(8,128)(2,1)} %fusion.4) | copy-start | bytes 1572868
  186.5 152.3 %copy-start.2 = (bf16[64,2048]{1,0:T(8,128)(2,1)S(1)}, bf16[64,2048]{1,0:T(8,128)(2,1)}, u32[]{:S(2)}) copy-start(bf16[64,2048]{1,0:T(8,128)(2,1)} %all_gather.26) | copy-start | bytes 786436
Sparse Core Ops, SparseCore 0:
  10.7 127.1 all-gather.4
  139.5 30.5 all-gather.6
  171.7 27.4 all-gather.8
  200.5 27.3 all-gather.10
  231.8 103.4 reduce-scatter.1
